TPU v7x, 32 devices: a whole 2x2x4 slice. The times are simulated.
32 devices in a mesh: fs: 8 (over z, y), tp: 4 (over x, core).
Axes of the slice: x: 2, y: 2, z: 4, core: 2. Of those that a mesh axis runs over, the one named last changes fastest.
Arguments:
- tokens: bfloat16 [8192, 2048], P('fs', 'tp'), may hold values from -6 to 6
- norm_gain: float32 [2048], P('fs'), may hold values from 0.1 to 1.9
- up_master: float32 [2048, 8192], P('fs', 'tp'), may hold values from -0.125 to 0.125
- down_master: float32 [2048, 8192], P('fs', 'tp'), may hold values from -0.0625 to 0.0625
Outputs:
- up_weights: bfloat16 [2048, 8192], P(None, 'tp')
- down_weights: bfloat16 [8192, 2048], P('tp')
- mlp_out: bfloat16 [8192, 2048], P('fs', 'tp')
All inputs are finite; a program needn't handle non-finite values.
Results may differ from a plain program's by a relative error of at most 0.014.
Values may be sent and summed in bfloat16 or wider, within the bound.
A program may use at most 128 MiB of HBM per device.

v0:
```python
import jax
import jax.numpy as jnp
from jax import lax
from jax.sharding import PartitionSpec as P

norm_floor = 1e-06


def on_device(tokens, norm_gain, up_master, down_master):
    up_local = (norm_gain[:, None] * up_master).astype(jnp.bfloat16)
    down_local = down_master.astype(jnp.bfloat16)
    gathered = lax.all_gather(tokens, "tp", axis=1, tiled=True)
    widened = gathered.astype(jnp.float32)
    normed = (
        widened * lax.rsqrt(jnp.mean(widened * widened, axis=-1, keepdims=True) + norm_floor)
    ).astype(jnp.bfloat16)
    up_whole, down_whole = (
        lax.all_gather(up_local, "fs", axis=0, tiled=True),
        lax.all_gather(down_local, "fs", axis=0, tiled=True),
    )
    preact = jnp.dot(normed, up_whole, preferred_element_type=jnp.float32)
    hidden = jnp.square(jax.nn.relu(preact)).astype(jnp.bfloat16)
    partial_value = jnp.einsum("tf,df->td", hidden, down_whole, preferred_element_type=jnp.float32)
    summed = lax.psum_scatter(
        partial_value.astype(jnp.bfloat16), "tp", scatter_dimension=1, tiled=True
    )
    return (up_whole, jnp.transpose(down_whole), summed)


def solution(mesh):
    in_specs = (P("fs", "tp"), P("fs"), P("fs", "tp"), P("fs", "tp"))
    out_specs = (P(None, "tp"), P("tp", None), P("fs", "tp"))
    return jax.shard_map(
        on_device, mesh=mesh, in_specs=in_specs, out_specs=out_specs, check_vma=False
    )
```

profile of v0, /device:TPU:0, one launch (start us, length us, event | category | flops | bytes accessed | tf_op | source)
XLA Modules:
  0.0 391.6 jit_solution(10137496696475460250)
XLA Ops:
  7.2 0.0 all-gather.8.cloned.1.call-start
  7.2 0.7 all-gather.8.cloned.1.call-update
  7.9 0.0 all-gather.4.cloned.1.call-start
  7.9 2.7 multiply_convert_fusion.1
  10.7 0.0 all-gather.4.cloned.1.call-update
  10.7 0.0 all-gather.6.cloned.1.call-start
  10.8 2.5 copy.7
  13.3 0.0 all-gather.6.cloned.1.call-update
  13.3 0.0 reduce-scatter.2.cloned.1.call-start
  13.4 33.4 %all-gather.8.cloned.1.call-done = bf16[1024,2048]{1,0:T(8,128)(2,1)} async-done(((bf16[1024,512]{1,0:T(8,128)(2,1)}), bf16[1024,2048]{1,0:T(8,128)(2,1)}) %all-gather.8.cloned.1.call-update) | async-done | bytes 4194320 | tf_op jit(solution)/shard_map/all_gather | solution.py:12
  46.7 3.1 fusion
  49.8 124.1 %all-gather.4.cloned.1.call-done = bf16[2048,2048]{1,0:T(8,128)(2,1)} async-done(((bf16[256,2048]{1,0:T(8,128)(2,1)}), bf16[2048,2048]{1,0:T(8,128)(2,1)}) %all-gather.4.cloned.1.call-update) | async-done | bytes 8388624 | tf_op jit(solution)/shard_map/all_gather | solution.py:18
  174.0 125.8 %all-gather.6.cloned.1.call-done = bf16[2048,2048]{0,1:T(8,128)(2,1)} async-done(((bf16[256,2048]{0,1:T(8,128)(2,1)}), bf16[2048,2048]{0,1:T(8,128)(2,1)}) %all-gather.6.cloned.1.call-update) | async-done | bytes 8388624 | tf_op jit(solution)/shard_map/all_gather | solution.py:19
  299.7 25.7 %fusion.9 = bf16[1024,2048]{1,0:T(8,128)(2,1)} fusion(bf16[2048,2048]{0,1:T(8,128)(2,1)} %all-gather.6.cloned.1.call-done, bf16[2048,2048]{1,0:T(8,128)(2,1)} %all-gather.4.cloned.1.call-done, bf16[1024,2048]{1,0:T(8,128)(2,1)} %all-gather.8.cloned.1.call-done, f32[1024]{0:T(1024)S(1)} %add_rsqrt_fusion), kind=kOutput, calls=%fused_computation.8 | convolution fusion | flops 17194549248 | bytes 25169920 | tf_op jit(solution)/shard_map/tf,df->td/dot_general | solution.py:23
  325.4 0.0 reduce-scatter.2.cloned.1.call-update
  325.5 42.7 %reduce-scatter.2.cloned.1.call-done = bf16[1024,512]{1,0:T(8,128)(2,1)} async-done(((bf16[1024,2048]{1,0:T(8,128)(2,1)}), bf16[1024,512]{1,0:T(8,128)(2,1)}) %reduce-scatter.2.cloned.1.call-update) | async-done | bytes 1048592 | tf_op jit(solution)/shard_map/reduce_scatter | solution.py:24
  368.2 8.4 %copy.10 = bf16[2048,2048]{1,0:T(8,128)(2,1)} copy(bf16[2048,2048]{1,0:T(8,128)(2,1)} %all-gather.4.cloned.1.call-done) | data formatting | bytes 16777216
  376.6 8.4 %copy.11 = bf16[2048,2048]{1,0:T(8,128)(2,1)} copy(bf16[2048,2048]{1,0:T(8,128)(2,1)} %bitcast.3) | data formatting | bytes 16777216
  (1 shorter events, 0.0 us)
Async XLA Ops:
  7.2 39.6 %all-gather.8.cloned.1.call-start = ((), (), s32[]{:S(2)}) async-start(), calls=%async_computation.3 | async-start | bytes 5242880 | tf_op jit(solution)/shard_map/all_gather | solution.py:12
  7.9 166.1 %all-gather.4.cloned.1.call-start = ((), (), s32[]{:S(2)}) async-start(), calls=%async_computation.1 | async-start | bytes 9437184 | tf_op jit(solution)/shard_map/all_gather | solution.py:18
  10.7 289.0 %all-gather.6.cloned.1.call-start = ((), (), s32[]{:S(2)}) async-start(), calls=%async_computation.2 | async-start | bytes 9437184 | tf_op jit(solution)/shard_map/all_gather | solution.py:19
  13.3 354.8 %reduce-scatter.2.cloned.1.call-start = ((), (), s32[]{:S(2)}) async-start(), calls=%async_computation.4 | async-start | bytes 5242880 | tf_op jit(solution)/shard_map/reduce_scatter | solution.py:24
Sparse Core Ops, SparseCore 0:
  9.5 37.1 all-gather.7
  49.4 124.4 all-gather.3
  176.6 123.1 all-gather.5
  325.6 42.5 reduce-scatter.1
where the time goes:
time: 392 us
  waiting for transfers between devices  327 us (83%)
  matrix products  25.7 us (7%)
  local copies, waits for them, and re-layouts  19.4 us (5%)
  between operations  13.8 us (4%)
  other arithmetic  5.82 us (1%)
    all_gather x1, waiting for transfers between devices, on_device(): lax.all_gather(down_local, 'fs', axis=0, tiled=True)  126 us
    all_gather x1, waiting for transfers between devices, on_device(): lax.all_gather(up_local, 'fs', axis=0, tiled=True)  124 us
    reduce_scatter x1, waiting for transfers between devices, on_device(): lax.psum_scatter(partial_value.astype(jnp.bfloat16), 'tp', scatter_dimens...  42.7 us
    all_gather x1, waiting for transfers between devices, on_device(): gathered = lax.all_gather(tokens, 'tp', axis=1, tiled=True)  33.4 us
    dot_general x1, matrix products, on_device(): jnp.einsum('tf,df->td', hidden, down_whole, preferred_element_type=jnp.fl...  25.7 us
    unnamed x3, local copies, waits for them, and re-layouts  19.4 us
  transfers between devices with their start and end apart: 4, of which 4 were waited for; matrix products, arithmetic and copies ran while one was open for 2% of the time, Pallas kernels for 0%

commit v1 on v0

--- a/solution.py
+++ b/solution.py
@@ -9,7 +9,12 @@
 def on_device(tokens, norm_gain, up_master, down_master):
     up_local = (norm_gain[:, None] * up_master).astype(jnp.bfloat16)
     down_local = down_master.astype(jnp.bfloat16)
-    gathered = lax.all_gather(tokens, "tp", axis=1, tiled=True)
+    ring = [tokens]
+    for hop in range(3):
+        ring.append(lax.ppermute(ring[-1], "tp", [(dev, (dev + 1) % 4) for dev in range(4)]))
+    gathered = jnp.roll(
+        jnp.concatenate(ring[::-1], axis=1), (lax.axis_index("tp") + 1) * ring[0].shape[1], axis=1
+    )
     widened = gathered.astype(jnp.float32)
     normed = (
         widened * lax.rsqrt(jnp.mean(widened * widened, axis=-1, keepdims=True) + norm_floor)

time: 392 us -> 356 us (0.908)
  waiting for transfers between devices: 327 us -> 285 us
  local copies, waits for them, and re-layouts: 19.4 us -> 26.5 us
    all_gather x1, waiting for transfers between devices: 124 us -> 73.6 us  [on_device(): lax.all_gather(up_local, 'fs', axis=0, tiled=True)]
    ppermute x0 -> x3, waiting for transfers between devices: none -> 42.9 us  [on_device(): lax.ppermute(ring[-1], 'tp', [(dev, (dev + 1) % 4) for dev in range(4)])]
    all_gather x1 -> x0, waiting for transfers between devices: 33.4 us -> none  [on_device(): gathered = lax.all_gather(tokens, 'tp', axis=1, tiled=True)]
    unnamed x3 -> x14, local copies, waits for them, and re-layouts: 19.4 us -> 26.4 us
  transfers between devices with their start and end apart: 4 -> 6, of which waited for: 4 -> 6; matrix products, arithmetic and copies ran while one was open for 2% -> 2% of each run, Pallas kernels for 0% -> 0%
where the time goes in v1:
time: 356 us
  waiting for transfers between devices  285 us (80%)
  local copies, waits for them, and re-layouts  26.5 us (7%)
  matrix products  25.7 us (7%)
  between operations  13.8 us (4%)
  other arithmetic  3.71 us (1%)
    all_gather x1, waiting for transfers between devices, on_device(): lax.all_gather(down_local, 'fs', axis=0, tiled=True)  126 us
    all_gather x1, waiting for transfers between devices, on_device(): lax.all_gather(up_local, 'fs', axis=0, tiled=True)  73.6 us
    ppermute x3, waiting for transfers between devices, on_device(): lax.ppermute(ring[-1], 'tp', [(dev, (dev + 1) % 4) for dev in range(4)])  42.9 us
    reduce_scatter x1, waiting for transfers between devices, on_device(): lax.psum_scatter(partial_value.astype(jnp.bfloat16), 'tp', scatter_dimens...  42.7 us
    unnamed x14, local copies, waits for them, and re-layouts  26.4 us
    dot_general x1, matrix products, on_device(): jnp.einsum('tf,df->td', hidden, down_whole, preferred_element_type=jnp.fl...  25.7 us
  transfers between devices with their start and end apart: 6, of which 6 were waited for; matrix products, arithmetic and copies ran while one was open for 2% of the time, Pallas kernels for 0%

profile of v1, /device:TPU:0, one launch (start us, length us, event | category | flops | bytes accessed | tf_op | source)
XLA Modules:
  0.0 355.5 jit_solution(90454146135864159)
XLA Ops:
  7.2 2.8 multiply_convert_fusion.1
  10.1 0.0 all-gather.5.cloned.1.call-start
  10.1 2.5 copy.7
  12.7 0.0 reduce-scatter.2.cloned.1.call-start
  12.7 0.5 collective-permute-start
  13.3 14.4 %collective-permute-done = bf16[1024,512]{1,0:T(8,128)(2,1)S(1)} collective-permute-done((bf16[1024,512]{1,0:T(8,128)(2,1)S(1)}, bf16[1024,512]{1,0:T(8,128)(2,1)S(1)}, u32[]{:S(2)}, u32[]{:S(2)}) %collective-permute-start) | collective-permute-done | bytes 1048608 | tf_op jit(solution)/shard_map/ppermute | solution.py:14
  27.7 14.2 %collective-permute-done.1 = bf16[1024,512]{1,0:T(8,128)(2,1)S(1)} collective-permute-done((bf16[1024,512]{1,0:T(8,128)(2,1)S(1)}, bf16[1024,512]{1,0:T(8,128)(2,1)S(1)}, u32[]{:S(2)}, u32[]{:S(2)}) %collective-permute-start.1) | collective-permute-done | bytes 1048608 | tf_op jit(solution)/shard_map/ppermute | solution.py:14
  41.9 14.3 %collective-permute-done.2 = bf16[1024,512]{1,0:T(8,128)(2,1)} collective-permute-done((bf16[1024,512]{1,0:T(8,128)(2,1)S(1)}, bf16[1024,512]{1,0:T(8,128)(2,1)}, u32[]{:S(2)}, u32[]{:S(2)}) %collective-permute-start.2) | collective-permute-done | bytes 1048608 | tf_op jit(solution)/shard_map/ppermute | solution.py:14
  56.2 1.4 constant_dynamic-update-slice_fusion.7
  57.6 0.2 constant_dynamic-update-slice_fusion.6
  57.8 0.2 constant_dynamic-update-slice_fusion.5
  57.9 0.2 constant_dynamic-update-slice_fusion.4
  58.1 1.4 constant_dynamic-update-slice_fusion.3
  59.5 0.2 constant_dynamic-update-slice_fusion.2
  59.7 0.2 constant_dynamic-update-slice_fusion.1
  59.8 0.2 constant_dynamic-update-slice_fusion
  60.0 3.4 copy-done.1
  63.4 0.9 fusion
  64.3 73.6 %all-gather.3.cloned.1.call-done = bf16[2048,2048]{1,0:T(8,128)(2,1)} async-done(((bf16[256,2048]{1,0:T(8,128)(2,1)}), bf16[2048,2048]{1,0:T(8,128)(2,1)}) %all-gather.3.cloned.1.call-update) | async-done | bytes 8388624 | tf_op jit(solution)/shard_map/all_gather | solution.py:23
  137.9 125.8 %all-gather.5.cloned.1.call-done = bf16[2048,2048]{0,1:T(8,128)(2,1)} async-done(((bf16[256,2048]{0,1:T(8,128)(2,1)}), bf16[2048,2048]{0,1:T(8,128)(2,1)}) %all-gather.5.cloned.1.call-update) | async-done | bytes 8388624 | tf_op jit(solution)/shard_map/all_gather | solution.py:24
  263.7 25.7 %fusion.9 = bf16[1024,2048]{1,0:T(8,128)(2,1)} fusion(bf16[2048,2048]{0,1:T(8,128)(2,1)} %all-gather.5.cloned.1.call-done, bf16[2048,2048]{1,0:T(8,128)(2,1)} %all-gather.3.cloned.1.call-done, f32[1024]{0:T(1024)S(1)} %add_rsqrt_fusion, bf16[1024,4096]{1,0:T(8,128)(2,1)} %copy-done.1, s32[]{:T(128)S(6)} %select_n.14), kind=kOutput, calls=%fused_computation.8 | convolution fusion | flops 17194549248 | bytes 25169924 | tf_op jit(solution)/shard_map/tf,df->td/dot_general | solution.py:28
  289.4 42.7 %reduce-scatter.2.cloned.1.call-done = bf16[1024,512]{1,0:T(8,128)(2,1)} async-done(((bf16[1024,2048]{1,0:T(8,128)(2,1)}), bf16[1024,512]{1,0:T(8,128)(2,1)}) %reduce-scatter.2.cloned.1.call-update) | async-done | bytes 1048592 | tf_op jit(solution)/shard_map/reduce_scatter | solution.py:29
  332.1 8.4 %copy.17 = bf16[2048,2048]{1,0:T(8,128)(2,1)} copy(bf16[2048,2048]{1,0:T(8,128)(2,1)} %all-gather.3.cloned.1.call-done) | data formatting | bytes 16777216
  340.6 8.4 %copy.18 = bf16[2048,2048]{1,0:T(8,128)(2,1)} copy(bf16[2048,2048]{1,0:T(8,128)(2,1)} %bitcast.3) | data formatting | bytes 16777216
  (10 shorter events, 0.1 us)
Async XLA Ops:
  7.2 5.6 %copy-start = (bf16[1024,512]{1,0:T(8,128)(2,1)S(1)}, bf16[1024,512]{1,0:T(8,128)(2,1)}, u32[]{:S(2)}) copy-start(bf16[1024,512]{1,0:T(8,128)(2,1)} %param.4) | copy-start | bytes 3145732
  7.2 130.7 %all-gather.3.cloned.1.call-start = ((), (), s32[]{:S(2)}) async-start(), calls=%async_computation.1 | async-start | bytes 9437184 | tf_op jit(solution)/shard_map/all_gather | solution.py:23
  10.1 253.6 %all-gather.5.cloned.1.call-start = ((), (), s32[]{:S(2)}) async-start(), calls=%async_computation.2 | async-start | bytes 9437184 | tf_op jit(solution)/shard_map/all_gather | solution.py:24
  12.7 319.4 %reduce-scatter.2.cloned.1.call-start = ((), (), s32[]{:S(2)}) async-start(), calls=%async_computation.3 | async-start | bytes 5242880 | tf_op jit(solution)/shard_map/reduce_scatter | solution.py:29
  12.7 14.9 %collective-permute-start = (bf16[1024,512]{1,0:T(8,128)(2,1)S(1)}, bf16[1024,512]{1,0:T(8,128)(2,1)S(1)}, u32[]{:S(2)}, u32[]{:S(2)}) collective-permute-start(bf16[1024,512]{1,0:T(8,128)(2,1)S(1)} %copy-done), channel_id=1, source_target_pairs={{0,1},{1,2},{2,3},{3,0},{4,5},{5,6},{6,7},{7,4},{8,9},{9,10},{10,1... | collective-permute-start | bytes 3145736 | tf_op jit(solution)/shard_map/ppermute | solution.py:14
  27.7 14.2 %collective-permute-start.1 = (bf16[1024,512]{1,0:T(8,128)(2,1)S(1)}, bf16[1024,512]{1,0:T(8,128)(2,1)S(1)}, u32[]{:S(2)}, u32[]{:S(2)}) collective-permute-start(bf16[1024,512]{1,0:T(8,128)(2,1)S(1)} %collective-permute-done), channel_id=1, source_target_pairs={{0,1},{1,2},{2,3},{3,0},{4,5},{5,6},{6,7},{7,4},{8,9},{9,10},{10,1... | collective-permute-start | bytes 3145736 | tf_op jit(solution)/shard_map/ppermute | solution.py:14
  41.9 14.3 %collective-permute-start.2 = (bf16[1024,512]{1,0:T(8,128)(2,1)S(1)}, bf16[1024,512]{1,0:T(8,128)(2,1)}, u32[]{:S(2)}, u32[]{:S(2)}) collective-permute-start(bf16[1024,512]{1,0:T(8,128)(2,1)S(1)} %collective-permute-done.1), channel_id=1, source_target_pairs={{0,1},{1,2},{2,3},{3,0},{4,5},{5,6},{6,7},{7,4},{8,9},{9,10},{10,1... | collective-permute-start | bytes 3145736 | tf_op jit(solution)/shard_map/ppermute | solution.py:14
  60.0 3.4 copy-start.1
Sparse Core Ops, SparseCore 0:
  10.7 127.1 all-gather.2
  140.5 123.1 all-gather.4
  289.5 42.5 reduce-scatter.1
